TPU v7x, 32 devices: a whole 2x2x4 slice. The times are simulated.
32 devices in a mesh: sp: 16 (over z, y, core), tp: 2 (over x).
Axes of the slice: x: 2, y: 2, z: 4, core: 2. Of those that a mesh axis runs over, the one named last changes fastest.
Arguments:
- pool_input: bfloat16 [4, 128, 8192], P(None, 'tp', 'sp'), may hold values from -8 to 8
- doc_ids: int32 [8192], P('sp'), may hold values from 0 to 3, never falling along the last dimension, each value on 1 to 4096 neighbouring positions
- pool_map: bfloat16 [4, 128, 128], replicated, may hold values from -0.5 to 0.5
- pool_scale: float32 [512], replicated, may hold values from 0.1 to 1.9
- w_out: bfloat16 [512, 2048], replicated, may hold values from -0.25 to 0.25
- residual: bfloat16 [8192, 2048], P(('sp', 'tp')), may hold values from -6 to 6
- mix_gain: float32 [2048], replicated, may hold values from 0.1 to 1.9
- ffn_gain: float32 [2048], replicated, may hold values from 0.1 to 1.9
- out_gain: float32 [2048], replicated, may hold values from 0.1 to 1.9
- expert_ids: int32 [8192, 2], P(('sp', 'tp')), may hold values from 0 to 31, all different within a row; in each aligned block of 256 rows (0 to 255, 256 to 511, ...) at most 32 rows name the same one
- route_logits: float32 [8192, 2], P(('sp', 'tp')), may hold values from -6 to 6
- w_gate: bfloat16 [32, 2048, 1024], P(('sp', 'tp')), may hold values from -0.125 to 0.125
- w_up: bfloat16 [32, 2048, 1024], P(('sp', 'tp')), may hold values from -0.125 to 0.125
- w_down: bfloat16 [32, 1024, 2048], P(('sp', 'tp')), may hold values from -0.1875 to 0.1875
Outputs:
- layer_out: bfloat16 [8192, 2048], P(('sp', 'tp'))
Inputs may be any that keep to these rules, and one draw needn't show every extreme that they name: `doc_ids`: document numbers never fall along the positions; no document has more than 4096 positions. `expert_ids`: each row names 2 different experts; within each aligned block of 256 rows no expert is named by more than 32 rows, a bound that some block reaches.
All inputs are finite; a program needn't handle non-finite values.
Results may differ from a plain program's by a relative error of at most 0.03.
Values may be sent and summed in bfloat16 or wider, within the bound.
A program may use at most 64 MiB of HBM per device.

v0:
```python
import jax
import jax.numpy as jnp
from jax import lax
from jax.sharding import PartitionSpec as P


def entering(value, axis, join, neutral):
    count, mine = (lax.axis_size(axis), lax.axis_index(axis))
    pieces = jax.tree.map(lambda part: lax.all_gather(part, axis), value)
    total = jax.tree.map(
        lambda part, zero: jnp.full_like(part, 0) + jnp.asarray(zero, part.dtype), value, neutral
    )

    def step(position, total):
        longer = join(total, jax.tree.map(lambda part: part[position], pieces))
        return jax.tree.map(lambda new, old: jnp.where(position < mine, new, old), longer, total)

    return lax.fori_loop(0, count - 1, step, total)


def passed_along(x, axis, by):
    devices = lax.axis_size(axis)
    pairs = [(i, i + by) for i in range(devices) if 0 <= i + by < devices]
    return lax.ppermute(x, axis, pairs)


def rms_scale(vector):
    return lax.rsqrt(jnp.mean(vector * vector, axis=-1, keepdims=True) + 1e-06)


def expert_rows(row_data, w_gate, w_up, w_down):
    gate_act = jnp.dot(row_data, w_gate[0], preferred_element_type=jnp.float32)
    up_act = jnp.dot(row_data, w_up[0], preferred_element_type=jnp.float32)
    hidden = (jax.nn.silu(gate_act) * up_act).astype(jnp.bfloat16)
    return jnp.dot(hidden, w_down[0], preferred_element_type=jnp.float32).astype(jnp.bfloat16)


def carry_combine(earlier, later):
    later_empty = later[2] < 0.0
    same_doc = earlier[2] == later[2]
    sums = jnp.where(later_empty, earlier[0], later[0] + jnp.where(same_doc, earlier[0], 0.0))
    counts = jnp.where(later_empty, earlier[1], later[1] + jnp.where(same_doc, earlier[1], 0.0))
    last_doc = jnp.where(later_empty, earlier[2], later[2])
    return (sums, counts, last_doc)


def local(
    pool_input,
    doc_ids,
    pool_map,
    pool_scale,
    w_out,
    residual,
    mix_gain,
    ffn_gain,
    out_gain,
    expert_ids,
    route_logits,
    w_gate,
    w_up,
    w_down,
):
    groups, channels, length = pool_input.shape
    values = pool_input.astype(jnp.float32)
    block_len = min(length, 128)
    block_count = length // block_len
    lower_tri = (jnp.arange(block_len)[:, None] <= jnp.arange(block_len)[None, :]).astype(
        jnp.float32
    )
    pieces = values.reshape(groups, channels, block_count, block_len)
    within = jnp.einsum("gcbk,kt->gcbt", pieces, lower_tri, precision=lax.Precision.HIGHEST)
    totals = within[..., -1]
    before_blocks = jnp.cumsum(totals, axis=2) - totals
    prefix = (within + before_blocks[..., None]).reshape(groups, channels, length)
    position = jnp.arange(length, dtype=jnp.int32)
    resets = jnp.concatenate([jnp.zeros((1,), bool), doc_ids[1:] != doc_ids[:-1]])
    starts = lax.cummax(jnp.where(resets, position, 0), axis=0)
    before = jnp.concatenate(
        [jnp.zeros((groups, channels, 1), jnp.float32), prefix[:, :, :-1]], axis=2
    )
    local_run = prefix - jnp.take(before, starts, axis=2)
    local_count = (position - starts + 1).astype(jnp.float32)
    last_id = doc_ids[-1].astype(jnp.float32)
    identity = (
        jnp.zeros((groups, channels), jnp.float32),
        jnp.zeros((), jnp.float32),
        jnp.full((), -1.0, jnp.float32),
    )
    carried = entering(
        (local_run[:, :, -1], local_count[-1], last_id), "sp", carry_combine, identity
    )
    joined = doc_ids.astype(jnp.float32) == carried[2]
    running = local_run + jnp.where(joined, carried[0][..., None], 0.0)
    doc_position = local_count + jnp.where(joined, carried[1], 0.0)
    diff_list = []
    for group_idx in range(groups):
        span_len = length * 2**group_idx
        far_rows = passed_along(
            running[group_idx].astype(jnp.bfloat16), "sp", 2**group_idx
        ).astype(jnp.float32)
        window = running[group_idx] - jnp.where(doc_position > span_len, far_rows, 0.0)
        window_mean = window / jnp.minimum(doc_position, float(span_len))
        diff_list.append((window_mean - values[group_idx]).astype(jnp.bfloat16))
    pool_diff = jnp.stack(diff_list)
    by_token = lax.all_to_all(pool_diff, "tp", split_axis=2, concat_axis=1, tiled=True)
    row_count = by_token.shape[2]
    mapped = jnp.einsum(
        "gct,gcd->tgd", by_token, pool_map, preferred_element_type=jnp.float32
    ).reshape(row_count, -1)
    mapped = (mapped * pool_scale).astype(jnp.bfloat16)
    projected = jnp.dot(mapped, w_out, preferred_element_type=jnp.float32)
    stream = (residual.astype(jnp.float32) + mix_gain * projected * rms_scale(projected)).astype(
        jnp.bfloat16
    )
    stream_back = stream.astype(jnp.float32)
    normed = (ffn_gain * stream_back * rms_scale(stream_back)).astype(jnp.bfloat16)
    top_count = expert_ids.shape[1]
    width = normed.shape[1]
    experts = w_gate.shape[0] * lax.axis_size("sp") * lax.axis_size("tp")
    capacity = max(2, 2 * row_count * top_count // experts)
    flat_expert = expert_ids.reshape(-1)
    onehot = (flat_expert[:, None] == jnp.arange(experts, dtype=jnp.int32)[None, :]).astype(
        jnp.int32
    )
    slot_rank = jnp.sum((jnp.cumsum(onehot, axis=0) - onehot) * onehot, axis=1)
    slot_index = flat_expert * capacity + slot_rank
    source_row = jnp.arange(row_count * top_count, dtype=jnp.int32) // top_count
    slot_row = jnp.full((experts * capacity,), row_count, jnp.int32).at[slot_index].set(source_row)
    padded = jnp.concatenate([normed, jnp.zeros((1, width), jnp.bfloat16)], axis=0)
    outgoing = padded[slot_row].reshape(experts, capacity, width)
    arrived = lax.all_to_all(outgoing, ("sp", "tp"), split_axis=0, concat_axis=0, tiled=True)
    finished = expert_rows(arrived.reshape(-1, width), w_gate, w_up, w_down).reshape(arrived.shape)
    results = lax.all_to_all(
        finished, ("sp", "tp"), split_axis=0, concat_axis=0, tiled=True
    ).reshape(-1, width)
    gathered = results[slot_index].astype(jnp.float32).reshape(row_count, top_count, width)
    weights = jax.nn.sigmoid(route_logits - route_logits[:, ::-1])
    expert_sum = jnp.sum(weights[..., None] * gathered, axis=1)
    return (stream_back + out_gain * expert_sum * rms_scale(expert_sum)).astype(jnp.bfloat16)


def solution(mesh):
    in_specs = (
        P(None, "tp", "sp"),
        P("sp"),
        P(),
        P(),
        P(),
        P(("sp", "tp"), None),
        P(),
        P(),
        P(),
        P(("sp", "tp"), None),
        P(("sp", "tp"), None),
        P(("sp", "tp"), None, None),
        P(("sp", "tp"), None, None),
        P(("sp", "tp"), None, None),
    )
    out_specs = P(("sp", "tp"), None)
    return jax.shard_map(local, mesh=mesh, in_specs=in_specs, out_specs=out_specs, check_vma=False)
```

profile of v0, /device:TPU:0, one launch (start us, length us, event | category | flops | bytes accessed | tf_op | source)
XLA Modules:
  0.0 397.7 jit_solution(14159232634341501602)
XLA Ops:
  2.1 1.3 copy.66
  5.0 2.4 concatenate.13
  7.4 3.7 gather_fusion
  11.1 2.3 copy.54
  14.8 23.2 %all-gather = f32[64,64,1]{1,2,0:T(1,128)S(1)} all-gather(f32[4,64,1]{1,2,0:T(1,128)S(1)} %copy.55), channel_id=2, replica_groups=mesh['sp'=16,'tp'=2] {'sp'}, dimensions={0}, use_global_device_ids=true | all-gather | bytes 17408 | tf_op jit(solution)/shard_map/all_gather | solution.py:9
  40.1 29.8 %all-reduce.4 = (f32[16]{0:T(128)S(1)}, f32[16]{0:T(128)S(1)}) all-reduce(f32[16]{0:T(128)S(1)} %convert_dynamic-update-slice_fusion, f32[16]{0:T(128)S(1)} %slice_dynamic-update-slice_fusion), channel_id=1, replica_groups=mesh['sp'=16,'tp'=2] {'sp'}, use_global_device_ids=true, to_apply=%add.2 | all-reduce | flops 32 | bytes 256
  69.9 54.2 %while.18 = (s32[]{:T(128)}, f32[4,64]{1,0:T(4,128)S(1)}, f32[]{:T(128)}, f32[]{:T(128)}, s32[]{:T(128)}, /*index=5*/f32[16]{0:T(128)S(1)}, f32[16,4,64]{2,1,0:T...) while((s32[]{:T(128)}, f32[4,64]{1,0:T(4,128)S(1)}, f32[]{:T(128)}, ...), condition=%wide.region_4.5_spmd.clone, body=%wide.region_3.4_spmd.clone.sunk | while | flops 1292 | bytes 3326 | solution.py:18
  125.5 1.9 collective-permute-start.1
  127.4 2.0 collective-permute-start
  129.4 1.9 collective-permute-start.2
  131.3 3.1 collective-permute-start.3
  138.8 2.4 scatter_custom_fusion
  144.7 3.6 all-to-all-start
  148.3 5.1 %all-to-all-done = bf16[2,2,32768]{2,1,0:T(2,128)(2,1)S(1)} async-done(((bf16[2,2,32768]{2,1,0:T(2,128)(2,1)}), bf16[2,2,32768]{2,1,0:T(2,128)(2,1)S(1)}, u32[]{:S(2)}, u32[]{:S(2)}) %all-to-all-start) | async-done | bytes 262176 | tf_op jit(solution)/shard_map/all_to_all | solution.py:105
  157.3 6.0 %gather_fusion.1 = bf16[1024,2048]{1,0:T(8,128)(2,1)} fusion(bf16[257,2048]{1,0:T(8,128)(2,1)S(1)} %concatenate.14, s32[1024]{0:T(1024)S(1)} %fusion.41), kind=kCustom, calls=%fused_computation.1 | custom fusion | bytes 8392704 | tf_op jit(solution)/shard_map/gather | solution.py:130
  163.4 96.9 %all_to_all.28 = bf16[32,32,2048]{2,1,0:T(8,128)(2,1)S(1)} all-to-all(bf16[32,32,2048]{2,1,0:T(8,128)(2,1)} %bitcast.186), channel_id=1, replica_groups=mesh['sp'=16,'tp'=2] {'sp','tp'}, dimensions={0} | all-to-all | bytes 8388608 | tf_op jit(solution)/shard_map/all_to_all | solution.py:131
  260.3 4.5 %fusion.2 = f32[1024,1024]{1,0:T(8,128)S(1)} fusion(bf16[1024,2048]{1,0:T(8,128)(2,1)S(1)} %bitcast.188, bf16[1,2048,1024]{2,1,0:T(8,128)(2,1)S(1)} %copy-done.12), kind=kOutput, calls=%fused_computation.8 | convolution fusion | flops 4294967296 | bytes 12582912 | tf_op jit(solution)/shard_map/dot_general | solution.py:33
  264.8 5.4 %multiply_convert_fusion = bf16[1024,1024]{1,0:T(8,128)(2,1)S(1)} fusion(f32[1024,1024]{1,0:T(8,128)S(1)} %fusion.2, bf16[1024,2048]{1,0:T(8,128)(2,1)S(1)} %bitcast.189, bf16[1,2048,1024]{2,1,0:T(8,128)(2,1)S(1)} %copy-done.13), kind=kOutput, calls=%fused_computation.13 | convolution fusion | flops 4301258752 | bytes 14680064 | tf_op jit(solution)/shard_map/dot_general | solution.py:32
  270.2 6.1 %fusion.6 = bf16[1024,2048]{1,0:T(8,128)(2,1)} fusion(bf16[1024,1024]{1,0:T(8,128)(2,1)S(1)} %multiply_convert_fusion, bf16[1,1024,2048]{2,1,0:T(8,128)(2,1)S(1)} %copy-done.14), kind=kOutput, calls=%fused_computation.14 | convolution fusion | flops 4297064448 | bytes 10485760 | tf_op jit(solution)/shard_map/dot_general | solution.py:35
  276.3 3.9 all-to-all-start.2
  280.5 93.2 %all-to-all-done.2 = bf16[32,32,2048]{2,1,0:T(8,128)(2,1)} async-done(((bf16[32,32,2048]{2,1,0:T(8,128)(2,1)}), bf16[32,32,2048]{2,1,0:T(8,128)(2,1)}, u32[]{:S(2)}, u32[]{:S(2)}) %all-to-all-start.2) | async-done | bytes 4194336 | tf_op jit(solution)/shard_map/all_to_all | solution.py:133
  373.7 8.0 %gather_fusion.2 = bf16[512,2048]{1,0:T(8,128)(2,1)} fusion(bf16[1024,2048]{1,0:T(8,128)(2,1)} %bitcast.36, s32[1024]{0:T(1024)S(1)} %pad_clamp_fusion), kind=kCustom, calls=%fused_computation.2 | custom fusion | bytes 4196352 | tf_op jit(solution)/shard_map/gather | solution.py:136
  381.7 5.4 %reshape.169 = f32[256,2,2048]{2,1,0:T(2,128)} reshape(bf16[512,2048]{1,0:T(8,128)(2,1)} %gather_fusion.2) | data formatting | bytes 6291456 | tf_op jit(solution)/shard_map/convert_element_type | solution.py:136
  387.1 9.0 %multiply_reduce_fusion = f32[256,2048]{1,0:T(8,128)S(1)} fusion(f32[256,2,2048]{2,1,0:T(2,128)} %reshape.169, f32[256,2]{1,0:T(8,128)S(1)} %copy.59), kind=kLoop, calls=%fused_computation.12 | loop fusion | flops 1572864 | bytes 6293504 | tf_op jit(solution)/shard_map/reduce_sum | solution.py:138
  (146 shorter events, 40.5 us)
Async XLA Ops:
  0.0 154.5 %copy-start = (bf16[512,2048]{1,0:T(8,128)(2,1)S(1)}, bf16[512,2048]{1,0:T(8,128)(2,1)}, u32[]{:S(2)}) copy-start(bf16[512,2048]{1,0:T(8,128)(2,1)} %param.20) | copy-start | bytes 6291460
  2.1 36.0 %copy-start.15 = (u32[32]{0:T(128)S(1)}, u32[32]{0:T(128)}, u32[]{:S(2)}) copy-start(u32[32]{0:T(128)} %constant.127) | copy-start | bytes 388
  2.1 36.6 %copy-start.6 = (s32[512]{0:T(512)S(1)}, s32[512]{0:T(512)}, u32[]{:S(2)}) copy-start(s32[512]{0:T(512)} %param.17) | copy-start | bytes 6148
  5.0 130.1 %copy-start.3 = (bf16[4,64,512]{2,1,0:T(8,128)(2,1)S(1)}, bf16[4,64,512]{2,1,0:T(8,128)(2,1)}, u32[]{:S(2)}) copy-start(bf16[4,64,512]{2,1,0:T(8,128)(2,1)} %param.16) | copy-start | bytes 786436
  124.8 29.3 %copy-start.5 = (bf16[4,128,128]{2,1,0:T(8,128)(2,1)S(1)}, bf16[4,128,128]{2,1,0:T(8,128)(2,1)}, u32[]{:S(2)}) copy-start(bf16[4,128,128]{2,1,0:T(8,128)(2,1)} %param.18) | copy-start | bytes 393220
  125.5 15.8 %collective-permute-start.1 = (bf16[64,512]{1,0:T(8,128)(2,1)}, bf16[64,512]{1,0:T(8,128)(2,1)}, u32[]{:S(2)}, u32[]{:S(2)}) collective-permute-start(bf16[64,512]{1,0:T(8,128)(2,1)} %get-tuple-element.207), channel_id=1, source_target_pairs={{0,4},{2,6},{4,8},{6,10},{8,12},{10,14},{12,16},{14,18},{16,20},{1... | collective-permute-start | bytes 196616 | tf_op jit(solution)/shard_map/ppermute | solution.py:24
  127.4 14.8 %collective-permute-start = (bf16[64,512]{1,0:T(8,128)(2,1)}, bf16[64,512]{1,0:T(8,128)(2,1)}, u32[]{:S(2)}, u32[]{:S(2)}) collective-permute-start(bf16[64,512]{1,0:T(8,128)(2,1)} %get-tuple-element.204), channel_id=1, source_target_pairs={{0,2},{2,4},{4,6},{6,8},{8,10},{10,12},{12,14},{14,16},{16,18},{18... | collective-permute-start | bytes 196616 | tf_op jit(solution)/shard_map/ppermute | solution.py:24
  129.4 12.7 %collective-permute-start.2 = (bf16[64,512]{1,0:T(8,128)(2,1)}, bf16[64,512]{1,0:T(8,128)(2,1)}, u32[]{:S(2)}, u32[]{:S(2)}) collective-permute-start(bf16[64,512]{1,0:T(8,128)(2,1)} %get-tuple-element.206), channel_id=1, source_target_pairs={{0,8},{2,10},{4,12},{6,14},{8,16},{10,18},{12,20},{14,22},{16,24},... | collective-permute-start | bytes 196616 | tf_op jit(solution)/shard_map/ppermute | solution.py:24
  131.3 10.8 %collective-permute-start.3 = (bf16[64,512]{1,0:T(8,128)(2,1)}, bf16[64,512]{1,0:T(8,128)(2,1)}, u32[]{:S(2)}, u32[]{:S(2)}) collective-permute-start(bf16[64,512]{1,0:T(8,128)(2,1)} %get-tuple-element.205), channel_id=1, source_target_pairs={{0,16},{2,18},{4,20},{6,22},{8,24},{10,26},{12,28},{14,30},{1,17},... | collective-permute-start | bytes 196616 | tf_op jit(solution)/shard_map/ppermute | solution.py:24
  135.1 19.3 %copy-start.11 = (f32[512]{0:T(512)S(1)}, f32[512]{0:T(512)}, u32[]{:S(2)}) copy-start(f32[512]{0:T(512)} %param.19) | copy-start | bytes 6148
  144.7 10.7 %copy-start.7 = (f32[2048]{0:T(1024)S(1)}, f32[2048]{0:T(1024)}, u32[]{:S(2)}) copy-start(f32[2048]{0:T(1024)} %param.22) | copy-start | bytes 24580
  144.7 8.7 %all-to-all-start = ((bf16[2,2,32768]{2,1,0:T(2,128)(2,1)}), bf16[2,2,32768]{2,1,0:T(2,128)(2,1)S(1)}, u32[]{:S(2)}, u32[]{:S(2)}) async-start(bf16[2,2,32768]{2,1,0:T(2,128)(2,1)} %reshape.220), calls=%async_computation | async-start | bytes 524288 | tf_op jit(solution)/shard_map/all_to_all | solution.py:105
  154.1 1.3 copy-start.4
  154.5 2.4 copy-start.8
  156.0 1.0 copy-start.1
  163.4 96.9 %copy-start.12 = (bf16[1,2048,1024]{2,1,0:T(8,128)(2,1)S(1)}, bf16[1,2048,1024]{2,1,0:T(8,128)(2,1)}, u32[]{:S(2)}) copy-start(bf16[1,2048,1024]{2,1,0:T(8,128)(2,1)} %param.28) | copy-start | bytes 12582916
  260.3 4.5 %copy-start.13 = (bf16[1,2048,1024]{2,1,0:T(8,128)(2,1)S(1)}, bf16[1,2048,1024]{2,1,0:T(8,128)(2,1)}, u32[]{:S(2)}) copy-start(bf16[1,2048,1024]{2,1,0:T(8,128)(2,1)} %param.27) | copy-start | bytes 12582916
  264.8 5.4 %copy-start.14 = (bf16[1,1024,2048]{2,1,0:T(8,128)(2,1)S(1)}, bf16[1,1024,2048]{2,1,0:T(8,128)(2,1)}, u32[]{:S(2)}) copy-start(bf16[1,1024,2048]{2,1,0:T(8,128)(2,1)} %param.29) | copy-start | bytes 12582916
  276.3 3.9 copy-start.10
  276.3 97.4 %all-to-all-start.2 = ((bf16[32,32,2048]{2,1,0:T(8,128)(2,1)}), bf16[32,32,2048]{2,1,0:T(8,128)(2,1)}, u32[]{:S(2)}, u32[]{:S(2)}) async-start(bf16[32,32,2048]{2,1,0:T(8,128)(2,1)} %bitcast.187), calls=%async_computation.2 | async-start | bytes 8388608 | tf_op jit(solution)/shard_map/all_to_all | solution.py:133
  387.1 9.2 %copy-start.2 = (bf16[256,2048]{1,0:T(8,128)(2,1)S(1)}, bf16[256,2048]{1,0:T(8,128)(2,1)}, u32[]{:S(2)}) copy-start(bf16[256,2048]{1,0:T(8,128)(2,1)} %copy-done.1) | copy-start | bytes 3145732
  387.1 9.2 %copy-start.9 = (f32[2048]{0:T(1024)S(1)}, f32[2048]{0:T(1024)}, u32[]{:S(2)}) copy-start(f32[2048]{0:T(1024)} %param.24) | copy-start | bytes 24580
where the time goes:
time: 399 us; the launch traced here: 398 us
  blocking collectives  150 us (38%)
  waiting for transfers between devices  98.3 us (25%)
  local copies, waits for them, and re-layouts  57.5 us (14%)
  loops' own time  35.5 us (9%)
  other arithmetic  21.1 us (5%)
  matrix products  18.4 us (5%)
  starting transfers between devices  16.5 us (4%)
    all_to_all x1, blocking collectives, local(): lax.all_to_all(outgoing, ('sp', 'tp'), split_axis=0, concat_axis=0, tiled...  96.9 us
    all_to_all x1, waiting for transfers between devices, local(): lax.all_to_all(finished, ('sp', 'tp'), split_axis=0, concat_axis=0, tiled...  93.2 us
    another operation x1, loops' own time, entering(): return lax.fori_loop(0, count - 1, step, total)  35.5 us
    unnamed x1, blocking collectives  29.8 us
    all_gather x1, blocking collectives, entering(): pieces = jax.tree.map(lambda part: lax.all_gather(part, axis), value)  23.2 us
    dynamic_slice x30, local copies, waits for them, and re-layouts, step(): longer = join(total, jax.tree.map(lambda part: part[position], pieces))  18.5 us
    ppermute x4, starting transfers between devices, passed_along(): return lax.ppermute(x, axis, pairs)  8.98 us
    reduce_sum x1, other arithmetic, local(): expert_sum = jnp.sum(weights[..., None] * gathered, axis=1)  8.96 us
  transfers between devices with their start and end apart: 6, of which 2 were waited for; matrix products, arithmetic and copies ran while one was open for 2% of the time, Pallas kernels for 0%

commit v1 on v0

v1 whole, which is shorter than its diff:
```python
import functools
import jax
import jax.numpy as jnp
from jax import lax
from jax.sharding import PartitionSpec as P
from jax.experimental import pallas as pl
from jax.experimental.pallas import tpu as pltpu

MESH = pl.DeviceIdType.MESH
EPS = 1e-06


def rms_scale(vector):
    return lax.rsqrt(jnp.mean(vector * vector, axis=-1, keepdims=True) + EPS)


def mixer_kernel(
    sp_count, tp_count,
    pool_ref, doc_ref, map_ref, scale_ref, w_out_ref, residual_ref, mix_ref, ffn_ref,
    stream_ref, normed_ref,
    tail_out, tails, run_out, far, diff_out, parts,
    tail_send, tail_recv, far_send, far_recv, diff_send, diff_recv,
):
    groups, channels, length = pool_ref.shape
    rows = length // tp_count
    lines = groups * channels
    sp, tp = lax.axis_index("sp"), lax.axis_index("tp")

    barrier = pltpu.get_barrier_semaphore()
    for i in range(1, sp_count):
        pl.semaphore_signal(
            barrier, inc=1, device_id=(lax.rem(sp + i, sp_count), tp), device_id_type=MESH
        )
    for i in range(1, tp_count):
        pl.semaphore_signal(
            barrier, inc=1, device_id=(sp, lax.rem(tp + i, tp_count)), device_id_type=MESH
        )

    values = pool_ref[...].reshape(lines, length)
    doc = doc_ref[...].astype(jnp.float32)
    last_id = doc[:, length - 1 :]
    tail_mask = jnp.broadcast_to((doc == last_id).astype(jnp.bfloat16), (8, length))
    tail_sum = lax.dot_general(
        tail_mask, values, (((1,), (1,)), ((), ())), preferred_element_type=jnp.float32
    )[:1]
    tail_count = jnp.sum((doc == last_id).astype(jnp.float32), axis=1, keepdims=True)
    tail_row = jnp.concatenate(
        [
            tail_sum,
            jnp.broadcast_to(last_id, (1, 128)),
            jnp.broadcast_to(tail_count, (1, 128)),
        ],
        axis=1,
    )
    tail_out[...] = tail_row
    tails[sp] = tail_row
    pl.semaphore_wait(barrier, sp_count + tp_count - 2)
    tail_copies = []
    for i in range(1, sp_count):
        copy = pltpu.make_async_remote_copy(
            src_ref=tail_out,
            dst_ref=tails.at[sp],
            send_sem=tail_send.at[i],
            recv_sem=tail_recv.at[i],
            device_id=(lax.rem(sp + i, sp_count), tp),
            device_id_type=MESH,
        )
        copy.start()
        tail_copies.append(copy)

    doc_col = jnp.broadcast_to(doc, (128, length)).T[:, :1]
    row_at = lax.broadcasted_iota(jnp.int32, (length, length), 0)
    col_at = lax.broadcasted_iota(jnp.int32, (length, length), 1)
    same = jnp.where((row_at <= col_at) & (doc_col == doc), 1.0, 0.0)
    local_count = jnp.sum(same, axis=0, keepdims=True)
    local_run = jnp.dot(values, same.astype(jnp.bfloat16), preferred_element_type=jnp.float32)

    for copy in tail_copies:
        copy.wait()
    table = jnp.concatenate([tails[j] for j in range(sp_count)], axis=0)
    sources = lax.broadcasted_iota(jnp.int32, (sp_count, 1), 0)
    joined = jnp.where(
        (sources < sp) & (table[:, lines : lines + 1] == doc), 1.0, 0.0
    )
    running = local_run + lax.dot_general(
        table[:, :lines],
        joined,
        (((0,), (0,)), ((), ())),
        preferred_element_type=jnp.float32,
        precision=lax.Precision.HIGHEST,
    )
    position = local_count + jnp.sum(
        joined * table[:, lines + 128 : lines + 129], axis=0, keepdims=True
    )
    run_out[...] = running.astype(jnp.bfloat16).reshape(groups, channels, length)
    far_copies = []
    for g in reversed(range(groups)):
        copy = pltpu.make_async_remote_copy(
            src_ref=run_out.at[g],
            dst_ref=far.at[g],
            send_sem=far_send.at[g],
            recv_sem=far_recv.at[g],
            device_id=(lax.rem(sp + 2**g, sp_count), tp),
            device_id_type=MESH,
        )
        copy.start()
        far_copies.append(copy)
    for copy in far_copies:
        copy.wait()
    for g in range(groups):
        span = float(length * 2**g)
        at = slice(g * channels, (g + 1) * channels)
        window = running[at] - jnp.where(position > span, far[g].astype(jnp.float32), 0.0)
        diff = window / jnp.minimum(position, span) - values[at].astype(jnp.float32)
        diff = diff.astype(jnp.bfloat16)
        for q in range(tp_count):
            diff_out[q, g] = diff[:, q * rows : (q + 1) * rows]
    parts[tp] = diff_out[tp]
    diff_copies = []
    for i in range(1, tp_count):
        other = lax.rem(tp + i, tp_count)
        copy = pltpu.make_async_remote_copy(
            src_ref=diff_out.at[other],
            dst_ref=parts.at[tp],
            send_sem=diff_send.at[i],
            recv_sem=diff_recv.at[i],
            device_id=(sp, other),
            device_id_type=MESH,
        )
        copy.start()
        diff_copies.append(copy)
    for copy in diff_copies:
        copy.wait()
    mapped = []
    for g in range(groups):
        channel_rows = jnp.concatenate([parts[q, g] for q in range(tp_count)], axis=0)
        mapped.append(
            lax.dot_general(
                channel_rows,
                map_ref[g],
                (((0,), (0,)), ((), ())),
                preferred_element_type=jnp.float32,
            )
        )
    mapped = (jnp.concatenate(mapped, axis=1) * scale_ref[...]).astype(jnp.bfloat16)
    projected = jnp.dot(mapped, w_out_ref[...], preferred_element_type=jnp.float32)
    stream = (
        residual_ref[...].astype(jnp.float32) + mix_ref[...] * projected * rms_scale(projected)
    ).astype(jnp.bfloat16)
    stream_ref[...] = stream
    back = stream.astype(jnp.float32)
    normed_ref[...] = (ffn_ref[...] * back * rms_scale(back)).astype(jnp.bfloat16)


def mixer(pool_input, doc_ids, pool_map, pool_scale, w_out, residual, mix_gain, ffn_gain):
    groups, channels, length = pool_input.shape
    sp_count, tp_count = lax.axis_size("sp"), lax.axis_size("tp")
    rows = length // tp_count
    tail_width = groups * channels + 256
    vmem = pl.BlockSpec(memory_space=pltpu.VMEM)
    shape = jax.ShapeDtypeStruct(residual.shape, jnp.bfloat16)
    return pl.pallas_call(
        functools.partial(mixer_kernel, sp_count, tp_count),
        out_shape=(shape, shape),
        in_specs=[vmem] * 8,
        out_specs=(vmem, vmem),
        scratch_shapes=[
            pltpu.VMEM((1, tail_width), jnp.float32),
            pltpu.VMEM((sp_count, 1, tail_width), jnp.float32),
            pltpu.VMEM((groups, channels, length), jnp.bfloat16),
            pltpu.VMEM((groups, channels, length), jnp.bfloat16),
            pltpu.VMEM((tp_count, groups, channels, rows), jnp.bfloat16),
            pltpu.VMEM((tp_count, groups, channels, rows), jnp.bfloat16),
            pltpu.SemaphoreType.DMA((sp_count,)),
            pltpu.SemaphoreType.DMA((sp_count,)),
            pltpu.SemaphoreType.DMA((groups,)),
            pltpu.SemaphoreType.DMA((groups,)),
            pltpu.SemaphoreType.DMA((tp_count,)),
            pltpu.SemaphoreType.DMA((tp_count,)),
        ],
        compiler_params=pltpu.CompilerParams(collective_id=0, has_side_effects=True),
    )(
        pool_input,
        doc_ids.reshape(1, -1),
        pool_map,
        pool_scale.reshape(1, -1),
        w_out,
        residual,
        mix_gain.reshape(1, -1),
        ffn_gain.reshape(1, -1),
    )


def expert_rows(row_data, w_gate, w_up, w_down):
    gate_act = jnp.dot(row_data, w_gate[0], preferred_element_type=jnp.float32)
    up_act = jnp.dot(row_data, w_up[0], preferred_element_type=jnp.float32)
    hidden = (jax.nn.silu(gate_act) * up_act).astype(jnp.bfloat16)
    return jnp.dot(hidden, w_down[0], preferred_element_type=jnp.float32).astype(jnp.bfloat16)


def slots_of(expert_ids, experts, capacity):
    rows = expert_ids.shape[0]
    ids = jnp.arange(experts, dtype=jnp.int32)
    chosen = (expert_ids[:, :, None] == ids).astype(jnp.float32)
    named = jnp.sum(chosen, axis=1)
    at = jnp.arange(rows)
    earlier = (at[:, None] > at[None, :]).astype(jnp.bfloat16)
    rank = jnp.dot(earlier, named.astype(jnp.bfloat16), preferred_element_type=jnp.float32)
    return expert_ids * capacity + jnp.sum(chosen * rank[:, None, :], axis=2).astype(jnp.int32)


def local(
    pool_input, doc_ids, pool_map, pool_scale, w_out, residual, mix_gain, ffn_gain, out_gain,
    expert_ids, route_logits, w_gate, w_up, w_down,
):
    row_count, top_count = expert_ids.shape
    width = residual.shape[1]
    experts = w_gate.shape[0] * lax.axis_size("sp") * lax.axis_size("tp")
    capacity = max(2, 2 * row_count * top_count // experts)
    slots = slots_of(expert_ids, experts, capacity)
    places = jnp.arange(experts * capacity, dtype=jnp.int32)
    picked = jnp.zeros((experts * capacity, row_count), jnp.bool_)
    for k in range(top_count):
        picked = picked | (places[:, None] == slots[:, k][None, :])
    picked = picked.astype(jnp.bfloat16)
    weights = jax.nn.sigmoid(route_logits - route_logits[:, ::-1])
    mix = jnp.zeros((row_count, experts * capacity), jnp.float32)
    for k in range(top_count):
        mix = mix + jnp.where(slots[:, k : k + 1] == places[None, :], weights[:, k : k + 1], 0.0)
    mix_high = mix.astype(jnp.bfloat16)
    mix_low = (mix - mix_high.astype(jnp.float32)).astype(jnp.bfloat16)

    stream, normed = mixer(
        pool_input, doc_ids, pool_map, pool_scale, w_out, residual, mix_gain, ffn_gain
    )
    outgoing = jnp.dot(picked, normed, preferred_element_type=jnp.float32).astype(jnp.bfloat16)
    outgoing = outgoing.reshape(experts, capacity, width)
    arrived = lax.all_to_all(outgoing, ("sp", "tp"), split_axis=0, concat_axis=0, tiled=True)
    finished = expert_rows(arrived.reshape(-1, width), w_gate, w_up, w_down).reshape(arrived.shape)
    results = lax.all_to_all(
        finished, ("sp", "tp"), split_axis=0, concat_axis=0, tiled=True
    ).reshape(-1, width)
    expert_sum = jnp.dot(mix_high, results, preferred_element_type=jnp.float32)
    expert_sum = expert_sum + jnp.dot(mix_low, results, preferred_element_type=jnp.float32)
    back = stream.astype(jnp.float32)
    return (back + out_gain * expert_sum * rms_scale(expert_sum)).astype(jnp.bfloat16)


def solution(mesh):
    rows = P(("sp", "tp"), None)
    cubes = P(("sp", "tp"), None, None)
    in_specs = (
        P(None, "tp", "sp"), P("sp"), P(), P(), P(), rows, P(), P(), P(), rows, rows,
        cubes, cubes, cubes,
    )
    return jax.shard_map(local, mesh=mesh, in_specs=in_specs, out_specs=rows, check_vma=False)
```

time: 399 us -> 252 us (0.63)
  local copies, waits for them, and re-layouts: 57.5 us -> 0.13 us
  blocking collectives: 150 us -> 95.6 us
  loops' own time: 35.5 us -> 0 us
  Pallas kernels: 0 us -> 29.2 us
  other arithmetic: 21.1 us -> 3.48 us
  starting transfers between devices: 16.5 us -> 3.89 us
  matrix products: 18.4 us -> 26.1 us
  waiting for transfers between devices: 98.3 us -> 93.3 us
    another operation x1 -> x0, loops' own time: 35.5 us -> none  [entering(): return lax.fori_loop(0, count - 1, step, total)]
    unnamed x1 -> x0, blocking collectives: 29.8 us -> none
    pallas_call x0 -> x1, Pallas kernels: none -> 29.2 us  [mixer(): pl.pallas_call(functools.partial(mixer_kernel, sp_count, tp_count), out_s...]
    all_gather x1 -> x0, blocking collectives: 23.2 us -> none  [entering(): pieces = jax.tree.map(lambda part: lax.all_gather(part, axis), value)]
    gather x4 -> x0, local copies, waits for them, and re-layouts: 20 us -> none  [the longest x1 8 us: local(): results[slot_index].astype(jnp.float32).reshape(row_count, top_count, width)]
    dynamic_slice x30 -> x0, local copies, waits for them, and re-layouts: 18.5 us -> none  [step(): longer = join(total, jax.tree.map(lambda part: part[position], pieces))]
    ppermute x4 -> x0, starting transfers between devices: 8.98 us -> none  [passed_along(): return lax.ppermute(x, axis, pairs)]
    reduce_sum x4 -> x2, other arithmetic: 9.87 us -> 1.43 us  [the longest x1 0.74 us: slots_of(): jnp.sum(chosen * rank[:, None, :], axis=2).astype(jnp.int32)]
  transfers between devices with their start and end apart: 6 -> 1, of which waited for: 2 -> 1; matrix products, arithmetic and copies ran while one was open for 2% -> 0% of each run, Pallas kernels for 0% -> 0%
where the time goes in v1:
time: 252 us
  blocking collectives  95.6 us (38%)
  waiting for transfers between devices  93.3 us (37%)
  Pallas kernels  29.2 us (12%)
  matrix products  26.1 us (10%)
  starting transfers between devices  3.89 us (2%)
  other arithmetic  3.48 us (1%)
    all_to_all x1, blocking collectives, local(): lax.all_to_all(outgoing, ('sp', 'tp'), split_axis=0, concat_axis=0, tiled...  95.6 us
    all_to_all x1, waiting for transfers between devices, local(): lax.all_to_all(finished, ('sp', 'tp'), split_axis=0, concat_axis=0, tiled...  93.3 us
    pallas_call x1, Pallas kernels, mixer(): pl.pallas_call(functools.partial(mixer_kernel, sp_count, tp_count), out_s...  29.2 us
    dot_general x1, matrix products, expert_rows(): jnp.dot(hidden, w_down[0], preferred_element_type=jnp.float32)  6.1 us
    dot_general x1, matrix products, expert_rows(): gate_act = jnp.dot(row_data, w_gate[0], preferred_element_type=jnp.float32)  5.35 us
  transfers between devices with their start and end apart: 1, of which 1 were waited for; matrix products, arithmetic and copies ran while one was open for 0% of the time, Pallas kernels for 0%

profile of v1, /device:TPU:0, one launch (start us, length us, event | category | flops | bytes accessed | tf_op | source)
XLA Modules:
  0.0 251.9 jit_solution(8108853677316903561)
XLA Ops:
  0.0 0.7 convert_reduce_fusion
  0.7 0.2 fusion.24
  0.8 0.7 select_reduce_fusion
  1.6 0.7 convert_add_fusion
  2.3 29.2 %shard_map.136 = (bf16[256,2048]{1,0:T(8,128)(2,1)}, bf16[256,2048]{1,0:T(8,128)(2,1)}) custom-call(bf16[4,64,512]{2,1,0:T(8,128)(2,1)} %pool_ref.1, s32[1,512]{1,0:T(1,128)} %bitcast.44, bf16[4,128,128]{2,1,0:T(8,128)(2,1)} %map_ref.1, f32[1,512]{1,0:T(1,128)} %bitcast.45, bf16[512,2048]{1,0:T(8,128)(2,1)} %w_out_ref.1, bf16[256,2048]{1,0:T(8,128)(2,1)} %residual_ref.1, ...), custom_call_target="tpu_custom_call" | custom-call | tf_op jit(solution)/shard_map/pallas_call | solution.py:162
  31.5 2.5 convolution_convert_fusion
  34.0 0.0 copy-start.3
  34.0 95.6 %all_to_all.10 = bf16[32,32,2048]{2,1,0:T(8,128)(2,1)S(1)} all-to-all(bf16[32,32,2048]{2,1,0:T(8,128)(2,1)S(1)} %bitcast.32), channel_id=1, replica_groups=mesh['sp'=16,'tp'=2] {'sp','tp'}, dimensions={0} | all-to-all | bytes 8388608 | tf_op jit(solution)/shard_map/all_to_all | solution.py:238
  129.6 0.0 copy-done.3
  129.6 4.5 %fusion.2 = f32[1024,1024]{1,0:T(8,128)S(1)} fusion(bf16[1024,2048]{1,0:T(8,128)(2,1)S(1)} %bitcast.34, bf16[1,2048,1024]{2,1,0:T(8,128)(2,1)S(1)} %copy-done.3), kind=kOutput, calls=%fused_computation.2 | convolution fusion | flops 4294967296 | bytes 12582912 | tf_op jit(solution)/shard_map/dot_general | solution.py:196
  134.1 0.0 copy-done.4
  134.1 0.0 copy-start.5
  134.2 5.4 %multiply_convert_fusion = bf16[1024,1024]{1,0:T(8,128)(2,1)S(1)} fusion(f32[1024,1024]{1,0:T(8,128)S(1)} %fusion.2, bf16[1024,2048]{1,0:T(8,128)(2,1)S(1)} %bitcast.35, bf16[1,2048,1024]{2,1,0:T(8,128)(2,1)S(1)} %copy-done.4), kind=kOutput, calls=%fused_computation.6 | convolution fusion | flops 4301258752 | bytes 14680064 | tf_op jit(solution)/shard_map/dot_general | solution.py:195
  139.5 0.0 copy-done.5
  139.5 6.1 %fusion.6 = bf16[1024,2048]{1,0:T(8,128)(2,1)} fusion(bf16[1024,1024]{1,0:T(8,128)(2,1)S(1)} %multiply_convert_fusion, bf16[1,1024,2048]{2,1,0:T(8,128)(2,1)S(1)} %copy-done.5), kind=kOutput, calls=%fused_computation.8 | convolution fusion | flops 4297064448 | bytes 10485760 | tf_op jit(solution)/shard_map/dot_general | solution.py:198
  145.6 3.9 %all-to-all-start.1 = ((bf16[32,32,2048]{2,1,0:T(8,128)(2,1)}), bf16[32,32,2048]{2,1,0:T(8,128)(2,1)}, u32[]{:S(2)}, u32[]{:S(2)}) async-start(bf16[32,32,2048]{2,1,0:T(8,128)(2,1)} %bitcast.33), calls=%async_computation.1 | async-start | bytes 8388608 | tf_op jit(solution)/shard_map/all_to_all | solution.py:240
  149.5 0.0 copy-done.2
  149.5 0.1 rev.3
  149.7 93.3 %all-to-all-done.1 = bf16[32,32,2048]{2,1,0:T(8,128)(2,1)} async-done(((bf16[32,32,2048]{2,1,0:T(8,128)(2,1)}), bf16[32,32,2048]{2,1,0:T(8,128)(2,1)}, u32[]{:S(2)}, u32[]{:S(2)}) %all-to-all-start.1) | async-done | bytes 4194336 | tf_op jit(solution)/shard_map/all_to_all | solution.py:240
  243.0 3.6 %fusion.22 = f32[256,2048]{1,0:T(8,128)S(1)} fusion(bf16[1024,2048]{1,0:T(8,128)(2,1)} %bitcast.14, f32[256]{0:T(256)S(1)} %bitcast.48, s32[256]{0:T(256)S(1)} %bitcast.40, f32[256]{0:T(256)S(1)} %bitcast.46, s32[256]{0:T(256)S(1)} %bitcast.37), kind=kOutput, calls=%fused_computation.27 | convolution fusion | flops 1075314688 | bytes 6295552 | tf_op jit(solution)/shard_map/dot_general | solution.py:243
  246.7 0.0 copy-start
  246.7 0.0 copy-start.1
  246.7 3.8 %multiply_reduce_fusion = (f32[256]{0:T(256)S(1)}, f32[256,2048]{1,0:T(8,128)S(1)}) fusion(f32[256,2048]{1,0:T(8,128)S(1)} %fusion.22, bf16[1024,2048]{1,0:T(8,128)(2,1)} %bitcast.14, f32[256]{0:T(256)S(1)} %bitcast.49, s32[256]{0:T(256)S(1)} %bitcast.41, f32[256]{0:T(256)S(1)} %bitcast.47, s32[256]{0:T(256)S(1)} %bitcast.38), kind=kOutput, calls=%fused_computation.11 | convolution fusion | flops 1077673728 | bytes 8393728 | tf_op jit(solution)/shard_map/dot_general | solution.py:244
  250.6 1.3 add_convert_fusion
  (8 shorter events, 0.0 us)
Async XLA Ops:
  34.0 95.7 %copy-start.3 = (bf16[1,2048,1024]{2,1,0:T(8,128)(2,1)S(1)}, bf16[1,2048,1024]{2,1,0:T(8,128)(2,1)}, u32[]{:S(2)}) copy-start(bf16[1,2048,1024]{2,1,0:T(8,128)(2,1)} %param.26) | copy-start | bytes 12582916
  129.6 4.5 %copy-start.4 = (bf16[1,2048,1024]{2,1,0:T(8,128)(2,1)S(1)}, bf16[1,2048,1024]{2,1,0:T(8,128)(2,1)}, u32[]{:S(2)}) copy-start(bf16[1,2048,1024]{2,1,0:T(8,128)(2,1)} %param.25) | copy-start | bytes 12582916
  134.1 5.4 %copy-start.5 = (bf16[1,1024,2048]{2,1,0:T(8,128)(2,1)S(1)}, bf16[1,1024,2048]{2,1,0:T(8,128)(2,1)}, u32[]{:S(2)}) copy-start(bf16[1,1024,2048]{2,1,0:T(8,128)(2,1)} %param.27) | copy-start | bytes 12582916
  145.6 3.9 %copy-start.2 = (f32[256,2]{0,1:T(2,128)S(1)}, f32[256,2]{0,1:T(2,128)}, u32[]{:S(2)}) copy-start(f32[256,2]{0,1:T(2,128)} %param.24) | copy-start | bytes 6148
  145.6 97.4 %all-to-all-start.1 = ((bf16[32,32,2048]{2,1,0:T(8,128)(2,1)}), bf16[32,32,2048]{2,1,0:T(8,128)(2,1)}, u32[]{:S(2)}, u32[]{:S(2)}) async-start(bf16[32,32,2048]{2,1,0:T(8,128)(2,1)} %bitcast.33), calls=%async_computation.1 | async-start | bytes 8388608 | tf_op jit(solution)/shard_map/all_to_all | solution.py:240
  246.7 3.9 %copy-start = (bf16[256,2048]{1,0:T(8,128)(2,1)S(1)}, bf16[256,2048]{1,0:T(8,128)(2,1)}, u32[]{:S(2)}) copy-start(bf16[256,2048]{1,0:T(8,128)(2,1)} %get-tuple-element.7) | copy-start | bytes 3145732
  246.7 3.9 %copy-start.1 = (f32[2048]{0:T(1024)S(1)}, f32[2048]{0:T(1024)}, u32[]{:S(2)}) copy-start(f32[2048]{0:T(1024)} %param.22) | copy-start | bytes 24580

commit v2 on v1

--- a/solution.py
+++ b/solution.py
@@ -198,7 +198,7 @@
     return jnp.dot(hidden, w_down[0], preferred_element_type=jnp.float32).astype(jnp.bfloat16)
 
 
-def slots_of(expert_ids, experts, capacity):
+def slots_of(expert_ids, experts, part):
     rows = expert_ids.shape[0]
     ids = jnp.arange(experts, dtype=jnp.int32)
     chosen = (expert_ids[:, :, None] == ids).astype(jnp.float32)
@@ -206,7 +206,9 @@
     at = jnp.arange(rows)
     earlier = (at[:, None] > at[None, :]).astype(jnp.bfloat16)
     rank = jnp.dot(earlier, named.astype(jnp.bfloat16), preferred_element_type=jnp.float32)
-    return expert_ids * capacity + jnp.sum(chosen * rank[:, None, :], axis=2).astype(jnp.int32)
+    rank = jnp.sum(chosen * rank[:, None, :], axis=2).astype(jnp.int32)
+    piece = rank // part
+    return (piece * experts + expert_ids) * part + rank - piece * part
 
 
 def local(
@@ -217,7 +219,9 @@
     width = residual.shape[1]
     experts = w_gate.shape[0] * lax.axis_size("sp") * lax.axis_size("tp")
     capacity = max(2, 2 * row_count * top_count // experts)
-    slots = slots_of(expert_ids, experts, capacity)
+    pieces = 2 if capacity % 2 == 0 else 1
+    part = capacity // pieces
+    slots = slots_of(expert_ids, experts, part)
     places = jnp.arange(experts * capacity, dtype=jnp.int32)
     picked = jnp.zeros((experts * capacity, row_count), jnp.bool_)
     for k in range(top_count):
@@ -233,15 +237,24 @@
     stream, normed = mixer(
         pool_input, doc_ids, pool_map, pool_scale, w_out, residual, mix_gain, ffn_gain
     )
-    outgoing = jnp.dot(picked, normed, preferred_element_type=jnp.float32).astype(jnp.bfloat16)
-    outgoing = outgoing.reshape(experts, capacity, width)
-    arrived = lax.all_to_all(outgoing, ("sp", "tp"), split_axis=0, concat_axis=0, tiled=True)
-    finished = expert_rows(arrived.reshape(-1, width), w_gate, w_up, w_down).reshape(arrived.shape)
-    results = lax.all_to_all(
-        finished, ("sp", "tp"), split_axis=0, concat_axis=0, tiled=True
-    ).reshape(-1, width)
-    expert_sum = jnp.dot(mix_high, results, preferred_element_type=jnp.float32)
-    expert_sum = expert_sum + jnp.dot(mix_low, results, preferred_element_type=jnp.float32)
+    axes = ("sp", "tp")
+    spans = [slice(i * experts * part, (i + 1) * experts * part) for i in range(pieces)]
+    arrived = []
+    for span in spans:
+        outgoing = jnp.dot(picked[span], normed, preferred_element_type=jnp.float32)
+        outgoing = outgoing.astype(jnp.bfloat16).reshape(experts, part, width)
+        arrived.append(lax.all_to_all(outgoing, axes, split_axis=0, concat_axis=0, tiled=True))
+    results = []
+    for rows in arrived:
+        finished = expert_rows(rows.reshape(-1, width), w_gate, w_up, w_down).reshape(rows.shape)
+        results.append(lax.all_to_all(finished, axes, split_axis=0, concat_axis=0, tiled=True))
+    expert_sum = jnp.zeros((row_count, width), jnp.float32)
+    for span, rows in zip(spans, results):
+        rows = rows.reshape(-1, width)
+        for share in (mix_high, mix_low):
+            expert_sum = expert_sum + jnp.dot(
+                share[:, span], rows, preferred_element_type=jnp.float32
+            )
     back = stream.astype(jnp.float32)
     return (back + out_gain * expert_sum * rms_scale(expert_sum)).astype(jnp.bfloat16)
 

time: 252 us -> 254 us (level)
  blocking collectives: 95.6 us -> 0 us
  waiting for transfers between devices: 93.3 us -> 155 us
  matrix products: 26.1 us -> 47.9 us
  starting transfers between devices: 3.89 us -> 14.2 us
  local copies, waits for them, and re-layouts: 0.13 us -> 2.77 us
    all_to_all x1 -> x0, blocking collectives: 95.6 us -> none  [local(): lax.all_to_all(outgoing, ('sp', 'tp'), split_axis=0, concat_axis=0, tiled...]
    all_to_all x1 -> x4, waiting for transfers between devices: 93.3 us -> 155 us  [the longest x2 78.2 us: local(): lax.all_to_all(outgoing, axes, split_axis=0, concat_axis=0, tiled=True)]
    dot_general x1 -> x2, matrix products: 6.1 us -> 21.1 us  [expert_rows(): jnp.dot(hidden, w_down[0], preferred_element_type=jnp.float32)]
    all_to_all x1 -> x4, starting transfers between devices: 3.89 us -> 14.2 us  [the longest x2 7.71 us: local(): lax.all_to_all(finished, axes, split_axis=0, concat_axis=0, tiled=True)]
    dot_general x1 -> x2, matrix products: 5.35 us -> 13 us  [expert_rows(): gate_act = jnp.dot(row_data, w_gate[0], preferred_element_type=jnp.float32)]
    unnamed x12, local copies, waits for them, and re-layouts: 0.03 us -> 2.68 us
    dot_general x4 -> x6, matrix products: 14.5 us -> 13.6 us  [the longest x4 8.26 us: local(): jnp.dot(share[:, span], rows, preferred_element_type=jnp.float32)]
  transfers between devices with their start and end apart: 1 -> 4, of which waited for: 1 -> 4; matrix products, arithmetic and copies ran while one was open for 0% -> 16% of each run, Pallas kernels for 0% -> 0%
where the time goes in v2:
time: 254 us; the launch traced here: 253 us
  waiting for transfers between devices  155 us (61%)
  matrix products  47.9 us (19%)
  Pallas kernels  29.3 us (12%)
  starting transfers between devices  14.2 us (6%)
  other arithmetic  4.04 us (2%)
  local copies, waits for them, and re-layouts  2.77 us (1%)
    all_to_all x2, waiting for transfers between devices, local(): lax.all_to_all(outgoing, axes, split_axis=0, concat_axis=0, tiled=True)  78.2 us
    all_to_all x2, waiting for transfers between devices, local(): lax.all_to_all(finished, axes, split_axis=0, concat_axis=0, tiled=True)  76.8 us
    pallas_call x1, Pallas kernels, mixer(): pl.pallas_call(functools.partial(mixer_kernel, sp_count, tp_count), out_s...  29.3 us
    dot_general x2, matrix products, expert_rows(): jnp.dot(hidden, w_down[0], preferred_element_type=jnp.float32)  21.1 us
    dot_general x2, matrix products, expert_rows(): gate_act = jnp.dot(row_data, w_gate[0], preferred_element_type=jnp.float32)  13 us
    dot_general x4, matrix products, local(): jnp.dot(share[:, span], rows, preferred_element_type=jnp.float32)  8.26 us
    all_to_all x2, starting transfers between devices, local(): lax.all_to_all(finished, axes, split_axis=0, concat_axis=0, tiled=True)  7.71 us
    all_to_all x2, starting transfers between devices, local(): lax.all_to_all(outgoing, axes, split_axis=0, concat_axis=0, tiled=True)  6.47 us
  transfers between devices with their start and end apart: 4, of which 4 were waited for; matrix products, arithmetic and copies ran while one was open for 16% of the time, Pallas kernels for 0%

profile of v2, /device:TPU:0, one launch (start us, length us, event | category | flops | bytes accessed | tf_op | source)
XLA Modules:
  0.0 253.4 jit_solution(6502750778107317406)
XLA Ops:
  0.8 0.7 select_reduce_fusion
  1.6 0.7 multiply_subtract_fusion
  2.5 29.3 %shard_map.136 = (bf16[256,2048]{1,0:T(8,128)(2,1)}, bf16[256,2048]{1,0:T(8,128)(2,1)}) custom-call(bf16[4,64,512]{2,1,0:T(8,128)(2,1)} %pool_ref.1, s32[1,512]{1,0:T(1,128)} %bitcast.70, bf16[4,128,128]{2,1,0:T(8,128)(2,1)} %map_ref.1, f32[1,512]{1,0:T(1,128)} %bitcast.71, bf16[512,2048]{1,0:T(8,128)(2,1)} %w_out_ref.1, bf16[256,2048]{1,0:T(8,128)(2,1)} %residual_ref.1, ...), custom_call_target="tpu_custom_call" | custom-call | tf_op jit(solution)/shard_map/pallas_call | solution.py:162
  31.8 3.3 %convolution_convert_fusion.1 = bf16[512,2048]{1,0:T(8,128)(2,1)} fusion(bf16[256,2048]{1,0:T(8,128)(2,1)} %get-tuple-element.8, pred[1024,256]{1,0:T(32,128)(4,1)S(1)} %fusion.23), kind=kOutput, calls=%fused_computation.15 | convolution fusion | flops 537919488 | bytes 3276800 | tf_op jit(solution)/shard_map/dot_general | solution.py:244
  35.2 2.9 %all-to-all-start = ((bf16[32,16,2048]{2,1,0:T(8,128)(2,1)}), bf16[32,16,2048]{2,1,0:T(8,128)(2,1)S(1)}, u32[]{:S(2)}, u32[]{:S(2)}) async-start(bf16[32,16,2048]{2,1,0:T(8,128)(2,1)} %bitcast.8), calls=%async_computation | async-start | bytes 4194304 | tf_op jit(solution)/shard_map/all_to_all | solution.py:246
  38.0 2.1 convolution_convert_fusion
  40.1 46.6 %all-to-all-done = bf16[32,16,2048]{2,1,0:T(8,128)(2,1)S(1)} async-done(((bf16[32,16,2048]{2,1,0:T(8,128)(2,1)}), bf16[32,16,2048]{2,1,0:T(8,128)(2,1)S(1)}, u32[]{:S(2)}, u32[]{:S(2)}) %all-to-all-start) | async-done | bytes 2097184 | tf_op jit(solution)/shard_map/all_to_all | solution.py:246
  86.7 1.3 copy-done.2
  88.0 3.6 %all-to-all-start.2 = ((bf16[32,16,2048]{2,1,0:T(8,128)(2,1)}), bf16[32,16,2048]{2,1,0:T(8,128)(2,1)S(1)}, u32[]{:S(2)}, u32[]{:S(2)}) async-start(bf16[32,16,2048]{2,1,0:T(8,128)(2,1)} %bitcast.15), calls=%async_computation.2 | async-start | bytes 4194304 | tf_op jit(solution)/shard_map/all_to_all | solution.py:246
  91.6 6.5 %fusion.10 = f32[512,1024]{1,0:T(8,128)} fusion(bf16[512,2048]{1,0:T(8,128)(2,1)} %bitcast.59, bf16[1,2048,1024]{2,1,0:T(8,128)(2,1)} %param.25), kind=kOutput, calls=%fused_computation.10 | convolution fusion | flops 2147483648 | bytes 8388608 | tf_op jit(solution)/shard_map/dot_general | solution.py:195
  98.1 10.6 %fusion.12 = bf16[512,2048]{1,0:T(8,128)(2,1)} fusion(bf16[1,1024,2048]{2,1,0:T(8,128)(2,1)} %param.27, f32[512,1024]{1,0:T(8,128)} %fusion.10, bf16[512,2048]{1,0:T(8,128)(2,1)} %bitcast.60, bf16[1,2048,1024]{2,1,0:T(8,128)(2,1)} %param.26), kind=kOutput, calls=%fused_computation.12 | convolution fusion | flops 4299161600 | bytes 14680064 | tf_op jit(solution)/shard_map/dot_general | solution.py:198
  108.7 31.6 %all-to-all-done.2 = bf16[32,16,2048]{2,1,0:T(8,128)(2,1)S(1)} async-done(((bf16[32,16,2048]{2,1,0:T(8,128)(2,1)}), bf16[32,16,2048]{2,1,0:T(8,128)(2,1)S(1)}, u32[]{:S(2)}, u32[]{:S(2)}) %all-to-all-start.2) | async-done | bytes 2097184 | tf_op jit(solution)/shard_map/all_to_all | solution.py:246
  140.3 1.3 copy-done.1
  141.6 3.9 %all-to-all-start.1 = ((bf16[32,16,2048]{2,1,0:T(8,128)(2,1)}), bf16[32,16,2048]{2,1,0:T(8,128)(2,1)S(1)}, u32[]{:S(2)}, u32[]{:S(2)}) async-start(bf16[32,16,2048]{2,1,0:T(8,128)(2,1)} %bitcast.61), calls=%async_computation.1 | async-start | bytes 4194304 | tf_op jit(solution)/shard_map/all_to_all | solution.py:250
  145.5 6.5 %fusion.8 = f32[512,1024]{1,0:T(8,128)} fusion(bf16[512,2048]{1,0:T(8,128)(2,1)} %bitcast.57, bf16[1,2048,1024]{2,1,0:T(8,128)(2,1)} %param.25), kind=kOutput, calls=%fused_computation.8 | convolution fusion | flops 2147483648 | bytes 8388608 | tf_op jit(solution)/shard_map/dot_general | solution.py:195
  152.0 10.6 %fusion.15 = bf16[512,2048]{1,0:T(8,128)(2,1)} fusion(bf16[1,1024,2048]{2,1,0:T(8,128)(2,1)} %param.27, f32[512,1024]{1,0:T(8,128)} %fusion.8, bf16[512,2048]{1,0:T(8,128)(2,1)} %bitcast.58, bf16[1,2048,1024]{2,1,0:T(8,128)(2,1)} %param.26), kind=kOutput, calls=%fused_computation.13 | convolution fusion | flops 4299161600 | bytes 14680064 | tf_op jit(solution)/shard_map/dot_general | solution.py:198
  162.6 31.4 %all-to-all-done.1 = bf16[32,16,2048]{2,1,0:T(8,128)(2,1)S(1)} async-done(((bf16[32,16,2048]{2,1,0:T(8,128)(2,1)}), bf16[32,16,2048]{2,1,0:T(8,128)(2,1)S(1)}, u32[]{:S(2)}, u32[]{:S(2)}) %all-to-all-start.1) | async-done | bytes 2097184 | tf_op jit(solution)/shard_map/all_to_all | solution.py:250
  194.0 3.8 %all-to-all-start.3 = ((bf16[32,16,2048]{2,1,0:T(8,128)(2,1)}), bf16[32,16,2048]{2,1,0:T(8,128)(2,1)}, u32[]{:S(2)}, u32[]{:S(2)}) async-start(bf16[32,16,2048]{2,1,0:T(8,128)(2,1)} %bitcast.56), calls=%async_computation.3 | async-start | bytes 4194304 | tf_op jit(solution)/shard_map/all_to_all | solution.py:250
  198.3 0.7 fusion.33
  199.0 2.1 convolution_add_fusion.2
  201.1 45.4 %all-to-all-done.3 = bf16[32,16,2048]{2,1,0:T(8,128)(2,1)} async-done(((bf16[32,16,2048]{2,1,0:T(8,128)(2,1)}), bf16[32,16,2048]{2,1,0:T(8,128)(2,1)}, u32[]{:S(2)}, u32[]{:S(2)}) %all-to-all-start.3) | async-done | bytes 2097184 | tf_op jit(solution)/shard_map/all_to_all | solution.py:250
  246.5 2.9 %convolution_add_fusion.1 = f32[256,2048]{1,0:T(8,128)S(1)} fusion(f32[256,2048]{1,0:T(8,128)} %convolution_add_fusion.2, bf16[512,2048]{1,0:T(8,128)(2,1)} %bitcast.18, bf16[256,1024]{1,0:T(8,128)(2,1)S(1)} %get-tuple-element.10), kind=kOutput, calls=%fused_computation.17 | convolution fusion | flops 537395200 | bytes 6553600 | tf_op jit(solution)/shard_map/dot_general | solution.py:255
  249.5 2.5 multiply_reduce_fusion
  252.0 1.3 add_convert_fusion
  (19 shorter events, 1.5 us)
Async XLA Ops:
  35.2 2.9 %copy-start = (bf16[256,2048]{1,0:T(8,128)(2,1)S(1)}, bf16[256,2048]{1,0:T(8,128)(2,1)}, u32[]{:S(2)}) copy-start(bf16[256,2048]{1,0:T(8,128)(2,1)} %get-tuple-element.8) | copy-start | bytes 3145732
  35.2 51.5 %all-to-all-start = ((bf16[32,16,2048]{2,1,0:T(8,128)(2,1)}), bf16[32,16,2048]{2,1,0:T(8,128)(2,1)S(1)}, u32[]{:S(2)}, u32[]{:S(2)}) async-start(bf16[32,16,2048]{2,1,0:T(8,128)(2,1)} %bitcast.8), calls=%async_computation | async-start | bytes 4194304 | tf_op jit(solution)/shard_map/all_to_all | solution.py:246
  86.7 1.3 copy-start.2
  88.0 52.3 %all-to-all-start.2 = ((bf16[32,16,2048]{2,1,0:T(8,128)(2,1)}), bf16[32,16,2048]{2,1,0:T(8,128)(2,1)S(1)}, u32[]{:S(2)}, u32[]{:S(2)}) async-start(bf16[32,16,2048]{2,1,0:T(8,128)(2,1)} %bitcast.15), calls=%async_computation.2 | async-start | bytes 4194304 | tf_op jit(solution)/shard_map/all_to_all | solution.py:246
  140.3 1.3 copy-start.1
  141.6 52.4 %all-to-all-start.1 = ((bf16[32,16,2048]{2,1,0:T(8,128)(2,1)}), bf16[32,16,2048]{2,1,0:T(8,128)(2,1)S(1)}, u32[]{:S(2)}, u32[]{:S(2)}) async-start(bf16[32,16,2048]{2,1,0:T(8,128)(2,1)} %bitcast.61), calls=%async_computation.1 | async-start | bytes 4194304 | tf_op jit(solution)/shard_map/all_to_all | solution.py:250
  194.0 3.8 %copy-start.5 = (f32[256,2]{0,1:T(2,128)S(1)}, f32[256,2]{0,1:T(2,128)}, u32[]{:S(2)}) copy-start(f32[256,2]{0,1:T(2,128)} %param.24) | copy-start | bytes 6148
  194.0 52.5 %all-to-all-start.3 = ((bf16[32,16,2048]{2,1,0:T(8,128)(2,1)}), bf16[32,16,2048]{2,1,0:T(8,128)(2,1)}, u32[]{:S(2)}, u32[]{:S(2)}) async-start(bf16[32,16,2048]{2,1,0:T(8,128)(2,1)} %bitcast.56), calls=%async_computation.3 | async-start | bytes 4194304 | tf_op jit(solution)/shard_map/all_to_all | solution.py:250
  249.5 2.6 %copy-start.3 = (bf16[256,2048]{1,0:T(8,128)(2,1)S(1)}, bf16[256,2048]{1,0:T(8,128)(2,1)}, u32[]{:S(2)}) copy-start(bf16[256,2048]{1,0:T(8,128)(2,1)} %get-tuple-element.7) | copy-start | bytes 3145732
  249.5 2.6 %copy-start.4 = (f32[2048]{0:T(1024)S(1)}, f32[2048]{0:T(1024)}, u32[]{:S(2)}) copy-start(f32[2048]{0:T(1024)} %param.22) | copy-start | bytes 24580
